TPU v7x, 32 devices: a whole 2x2x4 slice. The times are simulated.
32 devices in a mesh: sp: 8 (over z, core), tp: 4 (over y, x).
Axes of the slice: x: 2, y: 2, z: 4, core: 2. Of those that a mesh axis runs over, the one named last changes fastest.
Arguments:
- skip_path_vectors: bfloat16 [2048, 2048], P('sp'), may hold values from -10 to 10
- asker_raw_scores: bfloat16 [2048, 2048], P('sp', 'tp'), may hold values from -6 to 6
- retain_raw_scores: bfloat16 [2048, 2048], P('sp', 'tp'), may hold values from -5.5 to 5.5
- memory_write_entries: bfloat16 [2048, 2048], P('sp', 'tp'), may hold values from -6 to 6
- emit_switch_scores: bfloat16 [2048, 2048], P('sp', 'tp'), may hold values from -6 to 6
- retain_minimum_share: float32 [2048], P('tp'), may hold values from 0.88 to 0.99990234
- extra_shrink_rate: float32 [16, 2048], P('tp', 'sp'), may hold values from -0.7 to 0
- lane_rescale_factor: float32 [128], replicated, may hold values from 0.1 to 1.9
- emit_projection_array: bfloat16 [2048, 2048], P('tp'), may hold values from -0.1875 to 0.1875
- specialist_rescale_factor: float32 [2048], replicated, may hold values from 0.1 to 1.9
- specialist_switch_proj: bfloat16 [8, 2048, 4096], P('sp', None, 'tp'), may hold values from -0.125 to 0.125
- specialist_raise_proj: bfloat16 [8, 2048, 4096], P('sp', None, 'tp'), may hold values from -0.125 to 0.125
- specialist_lower_proj: bfloat16 [8, 4096, 2048], P('sp', 'tp'), may hold values from -0.375 to 0.375
- specialist_choice_ids: int32 [2048, 2], P('sp'), may hold values from 0 to 7, all different within a row; in each aligned block of 256 rows (0 to 255, 256 to 511, ...) at most 96 rows name the same one
- cluster_chance: float32 [2048], P('sp'), may hold values from 0.1 to 0.6
- specialist_duo_scores: float32 [2048, 2], P('sp'), may hold values from -2 to 2
Outputs:
- mixed_out: bfloat16 [2048, 2048], P('sp', 'tp')
Inputs may be any that keep to these rules, and one draw needn't show every extreme that they name: `specialist_choice_ids`: in each aligned block of 256 rows (the rows of one index of sp) no expert is named by more than 96 rows, a bound that some block reaches; the 2 ids of a row differ.
All inputs are finite; a program needn't handle non-finite values.
Results may differ from a plain program's by a relative error of at most 0.02.
Values may be sent and summed in bfloat16 or wider, within the bound.
A program may use at most 64 MiB of HBM per device.

v0:
```python
import jax
import jax.numpy as jnp
from jax import lax
from jax.sharding import PartitionSpec as P

EPS = 1e-06
PRECISE = lax.Precision.HIGHEST


def carried_in(array, axis, join, neutral):
    place = lax.axis_index(axis)
    gathered = jax.tree.map(
        lambda a, kind: lax.all_gather(a.astype(kind), axis), array, (jnp.bfloat16, jnp.bfloat16)
    )
    state = jax.tree.map(lambda a, e: jnp.zeros_like(a) + jnp.asarray(e, a.dtype), array, neutral)

    def one(lap, state):
        return join(
            state,
            jax.tree.map(
                lambda a, own: lax.dynamic_index_in_dim(a, lap, 0, False).astype(own.dtype),
                gathered,
                array,
            ),
        )

    return lax.fori_loop(0, place, one, state)


def chain_join(earlier, later):
    return (earlier[0] * later[0], later[0][:, :, None] * earlier[1] + later[1])


def rounded(float_value):
    return lax.optimization_barrier(float_value.astype(jnp.bfloat16)).astype(jnp.float32)


def fill_slots(rows, sources, places, slot_count):
    picked = rows[sources]
    return jnp.zeros((slot_count, rows.shape[1]), rows.dtype).at[places].set(picked)


def shards(
    skip_path_vectors,
    asker_raw_scores,
    retain_raw_scores,
    memory_write_entries,
    emit_switch_scores,
    retain_minimum_share,
    extra_shrink_rate,
    lane_rescale_factor,
    emit_projection_array,
    specialist_rescale_factor,
    specialist_switch_proj,
    specialist_raise_proj,
    specialist_lower_proj,
    specialist_choice_ids,
    cluster_chance,
    specialist_duo_scores,
):
    token_count_total = skip_path_vectors.shape[0]
    model_width = skip_path_vectors.shape[1]
    head_depth = lane_rescale_factor.shape[0]
    lanes_on_device = extra_shrink_rate.shape[0]
    retain_share = retain_minimum_share + (1.0 - retain_minimum_share) * jax.nn.sigmoid(
        retain_raw_scores.astype(jnp.float32)
    )
    retain_share = retain_share.reshape(token_count_total, lanes_on_device, head_depth)
    shrink_log_rate = jnp.log(retain_share) + extra_shrink_rate.T[:, :, None]
    key_rows = 1.0 - retain_share
    queries = jax.nn.silu(asker_raw_scores.astype(jnp.float32)).reshape(
        token_count_total, lanes_on_device, head_depth
    )
    values = memory_write_entries.astype(jnp.float32).reshape(
        token_count_total, lanes_on_device, head_depth
    )
    cumulative = jnp.cumsum(shrink_log_rate, axis=0)
    query_tilde = queries * jnp.exp(cumulative)
    key_tilde = key_rows * jnp.exp(-cumulative)
    causal = jnp.arange(token_count_total)[:, None] >= jnp.arange(token_count_total)[None, :]
    scores = jnp.einsum("thd,shd->hts", query_tilde, key_tilde, precision=PRECISE)
    scores = jnp.where(causal[None], scores, 0.0)
    inside = jnp.einsum("hts,shv->thv", scores, values, precision=PRECISE)
    totals = jnp.exp(cumulative[-1])
    own_state = jnp.einsum("shd,shv->hdv", key_tilde * totals[None], values, precision=PRECISE)
    identity = (jnp.ones_like(totals), jnp.zeros_like(own_state))
    carried = carried_in((totals, own_state), "sp", chain_join, identity)
    outside = jnp.einsum("thd,hdv->thv", query_tilde, carried[1], precision=PRECISE)
    readout = inside + outside
    normed_heads = readout * lax.rsqrt(jnp.mean(readout * readout, axis=-1, keepdims=True) + EPS)
    gated_out = (
        normed_heads
        * lane_rescale_factor
        * jax.nn.silu(
            emit_switch_scores.astype(jnp.float32).reshape(
                token_count_total, lanes_on_device, head_depth
            )
        )
    )
    mixer_out = gated_out.reshape(token_count_total, lanes_on_device * head_depth).astype(
        jnp.bfloat16
    )
    projected = rounded(
        jnp.dot(mixer_out, emit_projection_array, preferred_element_type=jnp.float32)
    )
    tp_size = lax.axis_size("tp")
    sp_size = lax.axis_size("sp")
    local_experts = specialist_switch_proj.shape[0]
    experts = local_experts * sp_size
    top_count = specialist_choice_ids.shape[1]
    capacity = 3 * token_count_total * top_count // (2 * experts)
    flat_ids = specialist_choice_ids.reshape(-1)
    matches = (flat_ids[:, None] == jnp.arange(experts, dtype=jnp.int32)[None, :]).astype(jnp.int32)
    before = jnp.cumsum(matches, axis=0) - matches
    places = flat_ids * capacity + jnp.sum(before * matches, axis=1)
    sources = jnp.arange(token_count_total * top_count, dtype=jnp.int32) // top_count
    col_width = model_width // tp_size
    col_start = lax.axis_index("tp") * col_width
    own_cols = lax.psum_scatter(
        projected.astype(jnp.bfloat16), "tp", scatter_dimension=1, tiled=True
    ).astype(jnp.float32)
    input_cols = lax.dynamic_slice_in_dim(skip_path_vectors, col_start, col_width, 1)
    resid_cols = (input_cols.astype(jnp.float32) + own_cols).astype(jnp.bfloat16)
    wide_rows = resid_cols.astype(jnp.float32)
    squares = lax.psum(jnp.sum(wide_rows * wide_rows, axis=1), "tp")
    gain_cols = lax.dynamic_slice_in_dim(specialist_rescale_factor, col_start, col_width, 0)
    normed = (wide_rows * lax.rsqrt(squares / model_width + EPS)[:, None] * gain_cols).astype(
        jnp.bfloat16
    )
    slot_rows = fill_slots(normed, sources, places, experts * capacity).reshape(
        experts, capacity, col_width
    )
    arrived = lax.all_to_all(slot_rows, "sp", split_axis=0, concat_axis=0, tiled=True)
    arrived = arrived.reshape(sp_size, local_experts, capacity, col_width)
    piece_cols = lax.all_gather(arrived, "tp", axis=3, tiled=True)
    gate_acts = jnp.einsum(
        "secd,edf->secf", piece_cols, specialist_switch_proj, preferred_element_type=jnp.float32
    )
    up_acts = jnp.einsum(
        "secd,edf->secf", piece_cols, specialist_raise_proj, preferred_element_type=jnp.float32
    )
    hidden = (jax.nn.silu(gate_acts) * up_acts).astype(jnp.bfloat16)
    part_out = rounded(
        jnp.einsum(
            "secf,efd->secd", hidden, specialist_lower_proj, preferred_element_type=jnp.float32
        )
    )
    summed = lax.psum_scatter(part_out.astype(jnp.bfloat16), "tp", scatter_dimension=3, tiled=True)
    returned = lax.all_to_all(
        summed.reshape(sp_size * local_experts, capacity, col_width),
        "sp",
        split_axis=0,
        concat_axis=0,
        tiled=True,
    )
    picked = returned.reshape(experts * capacity, col_width)[places].reshape(
        token_count_total, top_count, col_width
    )
    spread_logit = specialist_duo_scores[:, 0] - specialist_duo_scores[:, 1]
    weights = cluster_chance[:, None] * jnp.stack(
        [jax.nn.sigmoid(spread_logit), jax.nn.sigmoid(-spread_logit)], axis=1
    )
    mixed_out = resid_cols.astype(jnp.float32) + jnp.sum(
        weights[:, :, None] * picked.astype(jnp.float32), axis=1
    )
    return mixed_out.astype(jnp.bfloat16)


def solution(mesh):
    return jax.shard_map(
        shards,
        mesh=mesh,
        in_specs=(
            P("sp", None),
            P("sp", "tp"),
            P("sp", "tp"),
            P("sp", "tp"),
            P("sp", "tp"),
            P("tp"),
            P("tp", "sp"),
            P(),
            P("tp", None),
            P(),
            P("sp", None, "tp"),
            P("sp", None, "tp"),
            P("sp", "tp", None),
            P("sp", None),
            P("sp"),
            P("sp", None),
        ),
        out_specs=P("sp", "tp"),
        check_vma=False,
    )
```

profile of v0, /device:TPU:0, one launch (start us, length us, event | category | flops | bytes accessed | tf_op | source)
XLA Modules:
  0.0 271.8 jit_solution(15679918596882745785)
XLA Ops:
  6.5 1.2 copy.74
  7.8 0.7 broadcast_subtract_fusion.1
  8.5 0.9 broadcast_subtract_fusion
  9.4 1.6 add_bitcast_fusion
  11.0 2.1 copy.75
  13.0 1.4 fusion.31
  14.6 0.9 copy.77
  15.5 1.2 copy.78
  16.7 0.3 fusion.40
  17.0 1.1 convolution_convert_fusion.1
  18.1 0.0 reduce-scatter.3.cloned.1.call-start
  18.2 0.1 copy.82
  18.3 1.1 copy.73
  19.4 1.9 copy.86
  21.3 13.5 %all_gather.13 = bf16[8,4,128]{2,1,0:T(4,128)(2,1)S(1)} all-gather(bf16[1,4,128]{2,1,0:T(4,128)(2,1)S(1)} %copy.82), channel_id=1, replica_groups=mesh['sp'=8,'tp'=4] {'sp'}, dimensions={0}, use_global_device_ids=true | all-gather | bytes 9216 | tf_op jit(solution)/shard_map/all_gather | solution.py:13
  34.8 0.1 convert_multiply_fusion.2
  34.9 3.2 %convolution_select_fusion = f32[4,256,256]{2,1,0:T(8,128)} fusion(pred[256,256]{1,0:T(8,128)(4,1)S(1)} %iota_compare_fusion, f32[256,4,128]{0,2,1:T(8,128)S(1)} %bitcast.147, f32[256,4,128]{0,2,1:T(8,128)} %bitcast.150, f32[128,4,256]{2,0,1:T(8,128)S(1)} %copy.78), kind=kOutput, calls=%fused_computation.22 | convolution fusion | flops 403308544 | bytes 2686976 | tf_op jit(solution)/shard_map/thd,shd->hts/dot_general | solution.py:81
  38.1 5.1 %all-gather.5.cloned.1.call-done = bf16[32,128,128]{2,1,0:T(8,128)(2,1)} async-done(((bf16[4,128,128]{2,1,0:T(8,128)(2,1)}), bf16[32,128,128]{2,1,0:T(8,128)(2,1)}) %all-gather.5.cloned.1.call-update) | async-done | bytes 1048592 | tf_op jit(solution)/shard_map/all_gather | solution.py:13
  43.3 0.7 convolution_bitcast_fusion
  44.0 2.0 multiply_reduce_fusion.1
  46.0 0.2 multiply_convert_fusion
  46.2 1.7 convolution_convert_fusion
  48.0 0.1 copy.89
  48.2 0.1 eq.29
  48.3 0.1 eq.25
  48.5 1.1 reduce-window.16
  49.6 0.2 slice_reduce_fusion
  49.9 0.1 copy.88
  50.1 0.1 mul.156
  50.2 0.8 dynamic_slice.17
  51.0 0.1 fusion.45
  51.1 32.3 %reduce-scatter.3.cloned.1.call-done = bf16[256,512]{1,0:T(8,128)(2,1)} async-done(((bf16[256,2048]{1,0:T(8,128)(2,1)}), bf16[256,512]{1,0:T(8,128)(2,1)}) %reduce-scatter.3.cloned.1.call-update) | async-done | bytes 262160 | tf_op jit(solution)/shard_map/reduce_scatter | solution.py:119
  83.4 1.2 fusion.27
  84.6 8.9 %psum.7 = f32[256]{0:T(256)S(1)} all-reduce(f32[256]{0:T(256)S(1)} %get-tuple-element.77), channel_id=1, replica_groups=mesh['sp'=8,'tp'=4] {'tp'}, use_global_device_ids=true, to_apply=%region_10.11 | all-reduce | flops 256 | bytes 2048 | tf_op jit(solution)/shard_map/psum | solution.py:125
  93.5 0.1 fusion.29
  93.6 5.1 %scatter_custom_fusion = bf16[768,512]{1,0:T(8,128)(2,1)S(1)} fusion(s32[512]{0:T(512)S(1)} %bitcast.162, bf16[256,512]{1,0:T(8,128)(2,1)S(1)} %fusion.29, s32[1024]{0:T(1024)S(1)} %pad_clamp_fusion.1, bf16[]{:T(256)} %constant.78.clone.1), kind=kCustom, calls=%fused_computation.42 | custom fusion | bytes 786434 | tf_op jit(solution)/shard_map/scatter | solution.py:40
  98.8 25.5 %all_to_all.10 = bf16[8,96,512]{2,1,0:T(8,128)(2,1)} all-to-all(bf16[8,96,512]{2,1,0:T(8,128)(2,1)S(1)} %bitcast.151), channel_id=1, replica_groups=mesh['sp'=8,'tp'=4] {'sp'}, dimensions={0} | all-to-all | bytes 1572864 | tf_op jit(solution)/shard_map/all_to_all | solution.py:133
  124.3 41.8 %all-gather.7.cloned.1.call-done = bf16[8,96,2048]{2,1,0:T(8,128)(2,1)} async-done(((bf16[8,96,512]{2,1,0:T(8,128)(2,1)}), bf16[8,96,2048]{2,1,0:T(8,128)(2,1)}) %all-gather.7.cloned.1.call-update) | async-done | bytes 3145744 | tf_op jit(solution)/shard_map/all_gather | solution.py:135
  166.1 8.3 %fusion.2 = f32[8,96,1024]{2,1,0:T(8,128)} fusion(bf16[8,96,2048]{2,1,0:T(8,128)(2,1)} %all-gather.7.cloned.1.call-done, bf16[1,2048,1024]{2,1,0:T(8,128)(2,1)} %param.29), kind=kOutput, calls=%fused_computation.7 | convolution fusion | flops 3221225472 | bytes 10485760 | tf_op jit(solution)/shard_map/secd,edf->secf/dot_general | solution.py:139
  174.3 12.6 %fusion.13 = bf16[8,1,96,2048]{3,2,0,1:T(8,128)(2,1)} fusion(bf16[1,1024,2048]{2,1,0:T(8,128)(2,1)} %param.30, f32[8,96,1024]{2,1,0:T(8,128)} %fusion.2, bf16[8,96,2048]{2,1,0:T(8,128)(2,1)} %all-gather.7.cloned.1.call-done, bf16[1,2048,1024]{2,1,0:T(8,128)(2,1)} %param.28), kind=kOutput, calls=%fused_computation.19 | convolution fusion | flops 6448742400 | bytes 17825792 | tf_op jit(solution)/shard_map/secf,efd->secd/dot_general | solution.py:144
  187.0 44.1 %reduce-scatter.5.cloned.1.call-done = bf16[8,1,96,512]{3,2,0,1:T(8,128)(2,1)} async-done(((bf16[8,1,96,2048]{3,2,0,1:T(8,128)(2,1)}), bf16[8,1,96,512]{3,2,0,1:T(8,128)(2,1)}) %reduce-scatter.5.cloned.1.call-update) | async-done | bytes 786448 | tf_op jit(solution)/shard_map/reduce_scatter | solution.py:148
  231.0 4.6 %all-to-all-start.1 = ((bf16[8,96,512]{2,1,0:T(8,128)(2,1)}), bf16[8,96,512]{2,1,0:T(8,128)(2,1)S(1)}, u32[]{:S(2)}, u32[]{:S(2)}) async-start(bf16[8,96,512]{2,1,0:T(8,128)(2,1)} %bitcast.159), calls=%async_computation.3 | async-start | bytes 1572864 | tf_op jit(solution)/shard_map/all_to_all | solution.py:149
  235.7 0.1 copy.87
  235.8 20.7 %all-to-all-done.1 = bf16[8,96,512]{2,1,0:T(8,128)(2,1)S(1)} async-done(((bf16[8,96,512]{2,1,0:T(8,128)(2,1)}), bf16[8,96,512]{2,1,0:T(8,128)(2,1)S(1)}, u32[]{:S(2)}, u32[]{:S(2)}) %all-to-all-start.1) | async-done | bytes 786464 | tf_op jit(solution)/shard_map/all_to_all | solution.py:149
  256.6 2.6 gather_fusion
  259.2 2.7 reshape.237
  261.9 2.6 multiply_reduce_fusion
  264.5 0.8 fusion.30
  (43 shorter events, 0.5 us)
Async XLA Ops:
  6.5 39.7 %copy-start = (bf16[512,2048]{1,0:T(8,128)(2,1)S(1)}, bf16[512,2048]{1,0:T(8,128)(2,1)}, u32[]{:S(2)}) copy-start(bf16[512,2048]{1,0:T(8,128)(2,1)} %param.26) | copy-start | bytes 6291460
  6.5 36.7 %all-gather.5.cloned.1.call-start = ((), (), s32[]{:S(2)}) async-start(), calls=%async_computation.6 | async-start | bytes 1179648 | tf_op jit(solution)/shard_map/all_gather | solution.py:13
  9.4 7.6 %copy-start.1 = (f32[256,512]{0,1:T(8,128)}, f32[256,512]{0,1:T(8,128)S(1)}, u32[]{:S(2)}) copy-start(f32[256,512]{0,1:T(8,128)S(1)} %get-tuple-element.81) | copy-start | bytes 1572868
  9.4 7.6 %copy-start.3 = (bf16[256,512]{1,0:T(8,128)(2,1)S(1)}, bf16[256,512]{1,0:T(8,128)(2,1)}, u32[]{:S(2)}) copy-start(bf16[256,512]{1,0:T(8,128)(2,1)} %param.21) | copy-start | bytes 786436
  18.1 65.2 %reduce-scatter.3.cloned.1.call-start = ((), (), s32[]{:S(2)}) async-start(), calls=%async_computation.4 | async-start | bytes 1310720 | tf_op jit(solution)/shard_map/reduce_scatter | solution.py:119
  43.3 2.7 %copy-start.7 = (f32[128]{0:T(128)S(1)}, f32[128]{0:T(128)}, u32[]{:S(2)}) copy-start(f32[128]{0:T(128)} %param.25) | copy-start | bytes 1540
  43.3 2.7 copy-start.2
  46.0 2.0 copy-start.4
  48.0 118.1 %all-gather.7.cloned.1.call-start = ((), (), s32[]{:S(2)}) async-start(), calls=%async_computation.7 | async-start | bytes 3932160 | tf_op jit(solution)/shard_map/all_gather | solution.py:135
  124.3 106.8 %reduce-scatter.5.cloned.1.call-start = ((), (), s32[]{:S(2)}) async-start(), calls=%async_computation.5 | async-start | bytes 3932160 | tf_op jit(solution)/shard_map/reduce_scatter | solution.py:148
  186.9 48.7 %copy-start.5 = (f32[256,2]{0,1:T(2,128)S(1)}, f32[256,2]{0,1:T(2,128)}, u32[]{:S(2)}) copy-start(f32[256,2]{0,1:T(2,128)} %param.33) | copy-start | bytes 6148
  186.9 48.7 %copy-start.6 = (f32[256]{0:T(256)S(1)}, f32[256]{0:T(256)}, u32[]{:S(2)}) copy-start(f32[256]{0:T(256)} %param.32) | copy-start | bytes 3076
  231.0 25.6 %all-to-all-start.1 = ((bf16[8,96,512]{2,1,0:T(8,128)(2,1)}), bf16[8,96,512]{2,1,0:T(8,128)(2,1)S(1)}, u32[]{:S(2)}, u32[]{:S(2)}) async-start(bf16[8,96,512]{2,1,0:T(8,128)(2,1)} %bitcast.159), calls=%async_computation.3 | async-start | bytes 1572864 | tf_op jit(solution)/shard_map/all_to_all | solution.py:149
Sparse Core Ops, SparseCore 0:
  18.3 24.9 all-gather.4
  48.1 35.1 reduce-scatter.2
  124.4 41.6 all-gather.6
  187.1 43.8 reduce-scatter.4
where the time goes:
time: 273 us; the launch traced here: 272 us
  waiting for transfers between devices  144 us (53%)
  blocking collectives  47.9 us (18%)
  matrix products  29.5 us (11%)
  local copies, waits for them, and re-layouts  20.8 us (8%)
  between operations  13.4 us (5%)
  other arithmetic  11.4 us (4%)
  starting transfers between devices  4.74 us (2%)
    reduce_scatter x1, waiting for transfers between devices, shards(): lax.psum_scatter(part_out.astype(jnp.bfloat16), 'tp', scatter_dimension=3...  44.1 us
    all_gather x1, waiting for transfers between devices, shards(): piece_cols = lax.all_gather(arrived, 'tp', axis=3, tiled=True)  41.8 us
    reduce_scatter x1, waiting for transfers between devices, shards(): lax.psum_scatter(projected.astype(jnp.bfloat16), 'tp', scatter_dimension=...  32.3 us
    all_to_all x1, blocking collectives, shards(): lax.all_to_all(slot_rows, 'sp', split_axis=0, concat_axis=0, tiled=True)  25.5 us
    all_to_all x1, waiting for transfers between devices, shards(): lax.all_to_all(summed.reshape(sp_size * local_experts, capacity, col_widt...  20.7 us
    all_gather x1, blocking collectives, carried_in(): lax.all_gather(a.astype(kind), axis)  13.5 us
    dot_general x1, matrix products, shards(): jnp.einsum('secf,efd->secd', hidden, specialist_lower_proj, preferred_ele...  12.6 us
    psum x1, blocking collectives, shards(): squares = lax.psum(jnp.sum(wide_rows * wide_rows, axis=1), 'tp')  8.93 us
  transfers between devices with their start and end apart: 5, of which 5 were waited for; matrix products, arithmetic and copies ran while one was open for 4% of the time, Pallas kernels for 0%

commit v1 on v0

v1 whole, which is shorter than its diff:
```python
import functools

import jax
import jax.numpy as jnp
from jax import lax
from jax.experimental import pallas as pl
from jax.experimental.pallas import tpu as pltpu
from jax.sharding import PartitionSpec as P

EPS = 1e-06
PRECISE = lax.Precision.HIGHEST


MESH = pl.DeviceIdType.MESH
VMEM = pl.BlockSpec(memory_space=pltpu.VMEM)
VMEM_LIMIT = 60 * 1024 * 1024


def each(first, last, body):
    if last - first <= 8:
        for i in range(first, last):
            body(i)
    else:

        @pl.loop(first, last)
        def _(i):
            body(i)


def push(src, dst, send_sem, recv_sem, peer):
    return pltpu.make_async_remote_copy(
        src_ref=src,
        dst_ref=dst,
        send_sem=send_sem,
        recv_sem=recv_sem,
        device_id=peer,
        device_id_type=MESH,
    )


def state_kernel(sp_size, own_ref, out_ref, far_send, far_recv, near_send, near_recv):
    me = lax.axis_index("sp")
    pairs = sp_size // 2
    partner = me + 1 - 2 * lax.rem(me, 2)
    barrier = pltpu.get_barrier_semaphore()
    pl.semaphore_signal(barrier, inc=1, device_id={"sp": partner}, device_id_type=MESH)

    def far(d):
        return lax.rem(me + 2 * d, sp_size)

    def source(d):
        return lax.rem(me + sp_size - 2 * d, sp_size)

    def far_copy(d):
        return push(own_ref, out_ref.at[me], far_send.at[d], far_recv.at[d], {"sp": far(d)})

    def near_copy(d):
        block = own_ref if d is None else out_ref.at[source(d)]
        place = me if d is None else source(d)
        slot = 0 if d is None else d
        return push(
            block, out_ref.at[place], near_send.at[slot], near_recv.at[slot], {"sp": partner}
        )

    each(
        1,
        pairs,
        lambda d: pl.semaphore_signal(
            barrier, inc=1, device_id={"sp": far(d)}, device_id_type=MESH
        ),
    )
    pl.semaphore_wait(barrier, pairs)
    each(1, pairs, lambda d: far_copy(d).start())
    near_copy(None).start()

    def relay(d):
        far_copy(d).wait_recv()
        near_copy(d).start()

    each(1, pairs, relay)
    out_ref[me] = own_ref[...]
    near_copy(None).wait()

    def finish(d):
        far_copy(d).wait_send()
        near_copy(d).wait()

    each(1, pairs, finish)


def gather_states(packed):
    sp_size = lax.axis_size("sp")
    pairs = sp_size // 2
    dma = pltpu.SemaphoreType.DMA((pairs,))
    return pl.pallas_call(
        functools.partial(state_kernel, sp_size),
        out_shape=jax.ShapeDtypeStruct((sp_size,) + packed.shape, packed.dtype),
        in_specs=[VMEM],
        out_specs=VMEM,
        scratch_shapes=[dma, dma, dma, dma],
        compiler_params=pltpu.CompilerParams(collective_id=0, has_side_effects=True),
    )(packed)


def expert_kernel(
    sp_size,
    tp_size,
    group,
    mixer_ref,
    proj_ref,
    skip_ref,
    gain_ref,
    places_ref,
    gate_hbm,
    up_hbm,
    down_hbm,
    ret_ref,
    resid_ref,
    gate_w,
    up_w,
    down_w,
    pj,
    pj_in,
    sq,
    slots_in,
    slots,
    arr,
    part,
    got,
    hid,
    total,
    load_sem,
    pj_send,
    pj_recv,
    sq_send,
    sq_recv,
    out_send,
    out_recv,
    ag_send,
    ag_recv,
    rs_send,
    rs_recv,
    back_send,
    back_recv,
):
    my_s = lax.axis_index("sp")
    my_t = lax.axis_index("tp")
    tokens, width = skip_ref.shape
    cap = slots.shape[1]
    hidden_width = gate_w.shape[1]
    model_width = gate_w.shape[0]
    groups = sp_size // group
    rows = group * cap

    loads = [
        pltpu.make_async_copy(src, dst, load_sem.at[i])
        for i, (src, dst) in enumerate(((gate_hbm, gate_w), (up_hbm, up_w), (down_hbm, down_w)))
    ]
    barrier = pltpu.get_barrier_semaphore()

    def tp_of(j):
        return lax.rem(my_t + j, tp_size)

    def tp_from(j):
        return lax.rem(my_t + tp_size - j, tp_size)

    def sp_of(k):
        return lax.rem(my_s + k, sp_size)

    def sp_from(k):
        return lax.rem(my_s + sp_size - k, sp_size)

    each(
        1,
        tp_size,
        lambda j: pl.semaphore_signal(barrier, inc=1, device_id={"tp": tp_of(j)}, device_id_type=MESH),
    )
    each(
        1,
        sp_size,
        lambda k: pl.semaphore_signal(barrier, inc=1, device_id={"sp": sp_of(k)}, device_id_type=MESH),
    )
    for load in loads:
        load.start()

    def project(t):
        cols = pl.ds(pl.multiple_of(t * width, width), width)
        return jnp.dot(mixer_ref[...], proj_ref[:, cols], preferred_element_type=jnp.float32).astype(
            jnp.bfloat16
        )

    def pj_copy(j):
        return push(pj.at[j], pj_in.at[j], pj_send.at[j], pj_recv.at[j], {"tp": tp_of(j)})

    def project_all(j):
        pj[j] = project(tp_of(j))

    each(1, tp_size, project_all)
    pl.semaphore_wait(barrier, tp_size + sp_size - 2)
    each(1, tp_size, lambda j: pj_copy(j).start())
    total[...] = project(my_t).astype(jnp.float32)

    def add_in(j):
        pj_copy(j).wait_recv()
        total[...] += pj_in[j].astype(jnp.float32)

    each(1, tp_size, add_in)
    resid = (skip_ref[...].astype(jnp.float32) + total[...]).astype(jnp.bfloat16)
    resid_ref[...] = resid
    wide = resid.astype(jnp.float32)
    row_sums = jnp.sum(wide * wide, axis=1, keepdims=True)
    sq[0] = jnp.transpose(jnp.broadcast_to(row_sums, (tokens, 128)))[:8]

    def sq_copy(j):
        return push(sq.at[0], sq.at[j], sq_send.at[j], sq_recv.at[j], {"tp": tp_of(j)})

    each(1, tp_size, lambda j: sq_copy(j).start())
    slot_ids = lax.broadcasted_iota(jnp.int32, (sp_size * cap, tokens), 0)
    chosen = (slot_ids == places_ref[0:1, :]) | (slot_ids == places_ref[1:2, :])
    one_hot = chosen.astype(jnp.float32).astype(jnp.bfloat16)
    each(1, tp_size, lambda j: sq_copy(j).wait())
    squares = jnp.sum(sq[...], axis=0)[0:1]
    squares = jnp.transpose(jnp.broadcast_to(squares, (128, tokens)))[:, 0:1]
    normed = (wide * lax.rsqrt(squares / model_width + EPS) * gain_ref[...]).astype(jnp.bfloat16)
    filled = jnp.dot(one_hot, normed, preferred_element_type=jnp.float32).astype(jnp.bfloat16)
    slots_in[...] = filled.reshape(sp_size, cap, width)
    arr[my_t, 0] = filled[:cap]

    def out_copy(k):
        return push(
            slots_in.at[k], arr.at[my_t, k], out_send.at[k], out_recv.at[k], {"sp": sp_of(k)}
        )

    each(1, sp_size, lambda k: out_copy(k).start())

    def span(g):
        return pl.ds(g * group, group)

    def ag_copy(g, j):
        block = arr.at[my_t, span(g)]
        return push(block, block, ag_send.at[j, g], ag_recv.at[j, g], {"tp": tp_of(j)})

    def rs_copy(g, j):
        return push(
            part.at[j, span(g)],
            got.at[j, span(g)],
            rs_send.at[j, g],
            rs_recv.at[j, g],
            {"tp": tp_of(j)},
        )

    def back_copy(k):
        return push(
            slots.at[k], ret_ref.at[k], back_send.at[k], back_recv.at[k], {"sp": sp_from(k)}
        )


    def dispatch(g):
        def take(i):
            out_copy(g * group + i).wait_recv()

        each(1 if isinstance(g, int) and g == 0 else 0, group, take)
        each(1, tp_size, lambda j: ag_copy(g, j).start())

    dispatch(0)
    each(1, groups, dispatch)
    for load in loads:
        load.wait()
    tile = min(256, hidden_width)

    @pl.loop(0, groups)
    def _(g):
        each(1, tp_size, lambda j: ag_copy(g, j).wait_recv())

        @pl.loop(0, hidden_width // tile)
        def _(f):
            cols = pl.ds(pl.multiple_of(f * tile, tile), tile)
            gate = jnp.zeros((rows, tile), jnp.float32)
            up = jnp.zeros((rows, tile), jnp.float32)
            for t in range(tp_size):
                x = arr[t, span(g)].reshape(rows, width)
                depth = slice(t * width, (t + 1) * width)
                gate += jnp.dot(x, gate_w[depth, cols], preferred_element_type=jnp.float32)
                up += jnp.dot(x, up_w[depth, cols], preferred_element_type=jnp.float32)
            hid[:, cols] = (gate * jax.nn.sigmoid(gate) * up).astype(jnp.bfloat16)

        def lower(j):
            cols = pl.ds(pl.multiple_of(tp_of(j) * width, width), width)
            out = jnp.dot(hid[...], down_w[:, cols], preferred_element_type=jnp.float32)
            part[j, span(g)] = out.astype(jnp.bfloat16).reshape(group, cap, width)

        each(1, tp_size, lower)
        each(1, tp_size, lambda j: rs_copy(g, j).start())
        lower(0)

    def give_back(g):
        acc = part[0, span(g)].astype(jnp.float32)
        for j in range(1, tp_size):
            rs_copy(g, j).wait_recv()
            acc += got[j, span(g)].astype(jnp.float32)
        slots[span(g)] = acc.astype(jnp.bfloat16)
        each(
            1 if isinstance(g, int) and g == 0 else 0,
            group,
            lambda i: back_copy(g * group + i).start(),
        )

    give_back(0)
    each(1, groups, give_back)
    ret_ref[0] = slots[0]
    each(1, sp_size, lambda k: back_copy(k).wait())
    each(1, sp_size, lambda k: out_copy(k).wait_send())

    def drain(j):
        pj_copy(j).wait_send()
        for g in range(groups):
            ag_copy(g, j).wait_send()
            rs_copy(g, j).wait_send()

    each(1, tp_size, drain)


def run_experts(mixer_out, projection, skip_cols, gain_cols, places, gate, up, down, cap):
    sp_size = lax.axis_size("sp")
    tp_size = lax.axis_size("tp")
    tokens, width = skip_cols.shape
    model_width, hidden_width = gate.shape
    group = max(g for g in range(1, sp_size + 1) if sp_size % g == 0 and g * cap <= 256)
    groups = sp_size // group
    bf, f32 = jnp.bfloat16, jnp.float32
    dma = pltpu.SemaphoreType.DMA
    anywhere = pl.BlockSpec(memory_space=pl.ANY)
    return pl.pallas_call(
        functools.partial(expert_kernel, sp_size, tp_size, group),
        out_shape=(
            jax.ShapeDtypeStruct((sp_size, cap, width), bf),
            jax.ShapeDtypeStruct((tokens, width), bf),
        ),
        in_specs=[VMEM] * 5 + [anywhere] * 3,
        out_specs=(VMEM, VMEM),
        scratch_shapes=[
            pltpu.VMEM((model_width, hidden_width), bf),
            pltpu.VMEM((model_width, hidden_width), bf),
            pltpu.VMEM((hidden_width, model_width), bf),
            pltpu.VMEM((tp_size, tokens, width), bf),
            pltpu.VMEM((tp_size, tokens, width), bf),
            pltpu.VMEM((tp_size, 8, tokens), f32),
            pltpu.VMEM((sp_size, cap, width), bf),
            pltpu.VMEM((sp_size, cap, width), bf),
            pltpu.VMEM((tp_size, sp_size, cap, width), bf),
            pltpu.VMEM((tp_size, sp_size, cap, width), bf),
            pltpu.VMEM((tp_size, sp_size, cap, width), bf),
            pltpu.VMEM((group * cap, hidden_width), bf),
            pltpu.VMEM((tokens, width), f32),
            dma((3,)),
            dma((tp_size,)),
            dma((tp_size,)),
            dma((tp_size,)),
            dma((tp_size,)),
            dma((sp_size,)),
            dma((sp_size,)),
            dma((tp_size, groups)),
            dma((tp_size, groups)),
            dma((tp_size, groups)),
            dma((tp_size, groups)),
            dma((sp_size,)),
            dma((sp_size,)),
        ],
        compiler_params=pltpu.CompilerParams(
            collective_id=1, has_side_effects=True, vmem_limit_bytes=VMEM_LIMIT
        ),
    )(mixer_out, projection, skip_cols, gain_cols, places, gate, up, down)


def carry_states(totals, own_state):
    lanes, depth = totals.shape
    sp_size = lax.axis_size("sp")
    place = lax.axis_index("sp")
    pad = -lanes % 16
    packed = jnp.concatenate(
        [
            own_state.astype(jnp.bfloat16).reshape(lanes * depth, depth),
            totals.astype(jnp.bfloat16),
            jnp.zeros((pad, depth), jnp.bfloat16),
        ]
    )
    gathered = gather_states(packed)
    states = gathered[:, : lanes * depth].reshape(sp_size, lanes, depth, depth)
    shrinks = gathered[:, lanes * depth : lanes * depth + lanes].astype(jnp.float32)
    factor = jnp.ones((lanes, depth), jnp.float32)
    carried = jnp.zeros((lanes, depth, depth), jnp.float32)
    for lap in reversed(range(sp_size)):
        earlier = lap < place
        held = states[lap].astype(jnp.float32) * factor[:, :, None]
        carried = carried + jnp.where(earlier, held, 0.0)
        factor = jnp.where(earlier, factor * shrinks[lap], factor)
    return carried


def shards(
    skip_path_vectors,
    asker_raw_scores,
    retain_raw_scores,
    memory_write_entries,
    emit_switch_scores,
    retain_minimum_share,
    extra_shrink_rate,
    lane_rescale_factor,
    emit_projection_array,
    specialist_rescale_factor,
    specialist_switch_proj,
    specialist_raise_proj,
    specialist_lower_proj,
    specialist_choice_ids,
    cluster_chance,
    specialist_duo_scores,
):
    token_count_total = skip_path_vectors.shape[0]
    model_width = skip_path_vectors.shape[1]
    head_depth = lane_rescale_factor.shape[0]
    lanes_on_device = extra_shrink_rate.shape[0]
    retain_share = retain_minimum_share + (1.0 - retain_minimum_share) * jax.nn.sigmoid(
        retain_raw_scores.astype(jnp.float32)
    )
    retain_share = retain_share.reshape(token_count_total, lanes_on_device, head_depth)
    shrink_log_rate = jnp.log(retain_share) + extra_shrink_rate.T[:, :, None]
    key_rows = 1.0 - retain_share
    queries = jax.nn.silu(asker_raw_scores.astype(jnp.float32)).reshape(
        token_count_total, lanes_on_device, head_depth
    )
    values = memory_write_entries.astype(jnp.float32).reshape(
        token_count_total, lanes_on_device, head_depth
    )
    cumulative = jnp.cumsum(shrink_log_rate, axis=0)
    query_tilde = queries * jnp.exp(cumulative)
    key_tilde = key_rows * jnp.exp(-cumulative)
    causal = jnp.arange(token_count_total)[:, None] >= jnp.arange(token_count_total)[None, :]
    scores = jnp.einsum("thd,shd->hts", query_tilde, key_tilde, precision=PRECISE)
    scores = jnp.where(causal[None], scores, 0.0)
    inside = jnp.einsum("hts,shv->thv", scores, values, precision=PRECISE)
    totals = jnp.exp(cumulative[-1])
    own_state = jnp.einsum("shd,shv->hdv", key_tilde * totals[None], values, precision=PRECISE)
    carried = carry_states(totals, own_state)
    outside = jnp.einsum("thd,hdv->thv", query_tilde, carried, precision=PRECISE)
    readout = inside + outside
    normed_heads = readout * lax.rsqrt(jnp.mean(readout * readout, axis=-1, keepdims=True) + EPS)
    gated_out = (
        normed_heads
        * lane_rescale_factor
        * jax.nn.silu(
            emit_switch_scores.astype(jnp.float32).reshape(
                token_count_total, lanes_on_device, head_depth
            )
        )
    )
    mixer_out = gated_out.reshape(token_count_total, lanes_on_device * head_depth).astype(
        jnp.bfloat16
    )
    tp_size = lax.axis_size("tp")
    sp_size = lax.axis_size("sp")
    experts = sp_size
    top_count = specialist_choice_ids.shape[1]
    capacity = -(-3 * token_count_total * top_count // (2 * experts))
    capacity = -(-capacity // 16) * 16
    flat_ids = specialist_choice_ids.reshape(-1)
    matches = (flat_ids[:, None] == jnp.arange(experts, dtype=jnp.int32)[None, :]).astype(jnp.int32)
    before = jnp.cumsum(matches, axis=0) - matches
    turn = lax.rem(flat_ids + sp_size - lax.axis_index("sp"), sp_size)
    places = turn * capacity + jnp.sum(before * matches, axis=1)
    places = places.reshape(token_count_total, top_count)
    col_width = model_width // tp_size
    col_start = lax.axis_index("tp") * col_width
    skip_cols = lax.dynamic_slice_in_dim(skip_path_vectors, col_start, col_width, 1)
    gain_cols = lax.dynamic_slice_in_dim(specialist_rescale_factor, col_start, col_width, 0)
    returned, resid_cols = run_experts(
        mixer_out,
        emit_projection_array,
        skip_cols,
        gain_cols[None, :],
        places.T,
        specialist_switch_proj[0],
        specialist_raise_proj[0],
        specialist_lower_proj[0],
        capacity,
    )
    returned = returned.reshape(sp_size * capacity, col_width)
    slot_ids = jnp.arange(sp_size * capacity, dtype=jnp.int32)[None, :]
    picked = jnp.stack(
        [
            jnp.dot(
                (places[:, j : j + 1] == slot_ids).astype(jnp.bfloat16),
                returned,
                preferred_element_type=jnp.float32,
            )
            for j in range(top_count)
        ],
        axis=1,
    )
    spread_logit = specialist_duo_scores[:, 0] - specialist_duo_scores[:, 1]
    weights = cluster_chance[:, None] * jnp.stack(
        [jax.nn.sigmoid(spread_logit), jax.nn.sigmoid(-spread_logit)], axis=1
    )
    mixed_out = resid_cols.astype(jnp.float32) + jnp.sum(
        weights[:, :, None] * picked.astype(jnp.float32), axis=1
    )
    return mixed_out.astype(jnp.bfloat16)


def solution(mesh):
    return jax.shard_map(
        shards,
        mesh=mesh,
        in_specs=(
            P("sp", None),
            P("sp", "tp"),
            P("sp", "tp"),
            P("sp", "tp"),
            P("sp", "tp"),
            P("tp"),
            P("tp", "sp"),
            P(),
            P("tp", None),
            P(),
            P("sp", None, "tp"),
            P("sp", None, "tp"),
            P("sp", "tp", None),
            P("sp", None),
            P("sp"),
            P("sp", None),
        ),
        out_specs=P("sp", "tp"),
        check_vma=False,
    )
```

time: 273 us -> 153 us (0.56)
  waiting for transfers between devices: 144 us -> 0 us
  Pallas kernels: 0 us -> 121 us
  blocking collectives: 47.9 us -> 0 us
  matrix products: 29.5 us -> 7.53 us
  between operations: 13.4 us -> 0.41 us
  local copies, waits for them, and re-layouts: 20.8 us -> 13 us
  starting transfers between devices: 4.74 us -> 0 us
    pallas_call x0 -> x2, Pallas kernels: none -> 121 us  [the longest x1 103 us: run_experts(): pl.pallas_call(functools.partial(expert_kernel, sp_size, tp_size, group),...]
    reduce_scatter x2 -> x0, waiting for transfers between devices: 76.3 us -> none  [the longest x1 44.1 us: shards(): lax.psum_scatter(part_out.astype(jnp.bfloat16), 'tp', scatter_dimension=3...]
    all_gather x2 -> x0, waiting for transfers between devices: 46.9 us -> none  [the longest x1 41.8 us: shards(): piece_cols = lax.all_gather(arrived, 'tp', axis=3, tiled=True)]
    all_to_all x1 -> x0, blocking collectives: 25.5 us -> none  [shards(): lax.all_to_all(slot_rows, 'sp', split_axis=0, concat_axis=0, tiled=True)]
    all_to_all x1 -> x0, waiting for transfers between devices: 20.7 us -> none  [shards(): lax.all_to_all(summed.reshape(sp_size * local_experts, capacity, col_widt...]
    dot_general x4 -> x3, matrix products: 23.2 us -> 5.11 us  [the longest x2 3.13 us: shards(): jnp.dot((places[:, j:j + 1] == slot_ids).astype(jnp.bfloat16), returned,...]
    all_gather x1 -> x0, blocking collectives: 13.5 us -> none  [carried_in(): lax.all_gather(a.astype(kind), axis)]
    psum x1 -> x0, blocking collectives: 8.93 us -> none  [shards(): squares = lax.psum(jnp.sum(wide_rows * wide_rows, axis=1), 'tp')]
  transfers between devices with their start and end apart: 5 -> 0, of which waited for: 5 -> 0; matrix products, arithmetic and copies ran while one was open for 4% -> 0% of each run, Pallas kernels for 0% -> 0%
where the time goes in v1:
time: 153 us
  Pallas kernels  121 us (79%)
  local copies, waits for them, and re-layouts  13 us (8%)
  other arithmetic  10.4 us (7%)
  matrix products  7.53 us (5%)
    pallas_call x1, Pallas kernels, run_experts(): pl.pallas_call(functools.partial(expert_kernel, sp_size, tp_size, group),...  103 us
    pallas_call x1, Pallas kernels, gather_states(): pl.pallas_call(functools.partial(state_kernel, sp_size), out_shape=jax.Sh...  18.5 us
    convert_element_type x7, local copies, waits for them, and re-layouts, carry_states(): held = states[lap].astype(jnp.float32) * factor[:, :, None]  4.54 us
    dot_general x2, matrix products, shards(): jnp.dot((places[:, j:j + 1] == slot_ids).astype(jnp.bfloat16), returned,...  3.13 us

profile of v1, /device:TPU:0, one launch (start us, length us, event | category | flops | bytes accessed | tf_op | source)
XLA Modules:
  0.0 152.7 jit_solution(14481069306177626628)
XLA Ops:
  0.0 1.2 copy.54
  1.2 0.7 broadcast_subtract_fusion.1
  1.9 0.9 broadcast_subtract_fusion
  2.8 0.7 add_bitcast_fusion
  3.5 0.2 copy.55
  3.7 0.4 fusion.7
  4.2 0.1 copy.57
  4.4 0.2 copy.79
  4.7 0.1 copy.52
  4.8 0.1 convert_multiply_fusion
  5.0 0.2 copy.78
  5.2 1.2 broadcast_multiply_fusion
  6.4 0.7 convolution_convert_fusion
  7.1 0.8 maximum_maximum_fusion.own_ref
  7.9 18.5 %shard_map.154 = bf16[8,528,128]{2,1,0:T(8,128)(2,1)} custom-call(bf16[528,128]{1,0:T(8,128)(2,1)} %maximum_maximum_fusion.own_ref), custom_call_target="tpu_custom_call" | custom-call | tf_op jit(solution)/shard_map/pallas_call | solution.py:95
  26.4 0.7 slice_convert_fusion
  27.2 0.6 multiply_select_fusion
  27.7 0.9 convert_select_fusion
  28.7 0.1 copy.65
  28.8 2.0 %fusion.66 = (bf16[1,512,128]{2,1,0:T(8,128)(2,1)S(1)}, bf16[1,512,128]{2,1,0:T(8,128)(2,1)S(1)}, bf16[1,512,128]{2,1,0:T(8,128)(2,1)}, bf16[1,512,128]{2,1,0:T(...) fusion(bf16[8,528,128]{2,1,0:T(8,128)(2,1)} %shard_map.154), kind=kLoop, calls=%fused_computation.118 | loop fusion | bytes 1835008 | tf_op jit(solution)/shard_map/slice | solution.py:394
  30.8 0.1 copy.64
  30.9 0.1 copy.66
  31.0 0.1 copy.67
  31.1 0.8 copy.68
  31.9 0.8 copy.69
  32.8 1.8 %copy.70 = f32[4,128,128]{1,2,0:T(8,128)} copy(bf16[4,128,128]{2,1,0:T(8,128)(2,1)} %bitcast.131) | data formatting | bytes 393216 | tf_op jit(solution)/shard_map/convert_element_type | solution.py:394
  34.5 0.8 copy.71
  35.3 2.0 %convolution_bitcast_fusion = f32[256,4,128]{0,2,1:T(8,128)S(1)} fusion(f32[256,4,128]{2,1,0:T(4,128)S(1)} %get-tuple-element.27, f32[4,128,128]{1,2,0:T(8,128)} %copy.71, f32[4,128,128]{1,2,0:T(8,128)} %copy.70, f32[4,128,128]{1,2,0:T(8,128)} %copy.69, f32[4,128,128]{1,2,0:T(8,128)} %copy.68, f32[4,128,128]{1,2,0:T(8,128)S(1)} %copy.67, ...), kind=kOutput, calls=%fused_computation.1 | convolution fusion | flops 202702848 | bytes 3160071 | tf_op jit(solution)/shard_map/thd,hdv->thv/dot_general | solution.py:444
  37.4 1.0 convolution_select_fusion
  38.4 0.7 multiply_reduce_fusion
  39.2 0.2 copy-done.3
  39.4 0.1 copy.73
  39.5 0.2 multiply_convert_fusion
  39.7 0.8 copy.80.mixer_ref
  40.5 0.1 copy.75
  40.7 0.1 eq.59
  40.8 1.3 reduce-window.16
  42.2 0.2 slice_reduce_fusion
  42.4 0.1 eq.55
  42.7 0.1 reduce_sum.31
  42.9 0.6 fusion.58
  43.5 0.7 constant_dynamic-slice_fusion.skip_ref
  44.2 1.3 dynamic_slice.7
  45.6 102.9 %shard_map.155 = (bf16[8,96,512]{2,1,0:T(8,128)(2,1)}, bf16[256,512]{1,0:T(8,128)(2,1)}) custom-call(bf16[256,512]{1,0:T(8,128)(2,1)} %copy.80.mixer_ref, bf16[512,2048]{1,0:T(8,128)(2,1)} %proj_ref.1, bf16[256,512]{1,0:T(8,128)(2,1)} %constant_dynamic-slice_fusion.skip_ref, f32[1,512]{1,0:T(1,128)} %bitcast.140, s32[2,256]{1,0:T(2,128)} %bitcast.138, ...), custom_call_target="tpu_custom_call" | custom-call | tf_op jit(solution)/shard_map/pallas_call | solution.py:333
  148.6 1.6 %convolution_bitcast_fusion.3 = f32[256,1,512]{2,0,1:T(8,128)S(1)} fusion(bf16[768,512]{1,0:T(8,128)(2,1)} %bitcast.118, s32[256]{0:T(256)S(1)} %bitcast.143), kind=kOutput, calls=%fused_computation.5 | convolution fusion | flops 201523200 | bytes 1311744 | tf_op jit(solution)/shard_map/dot_general | solution.py:490
  150.2 1.5 %convolution_bitcast_fusion.2 = f32[256,1,512]{2,0,1:T(8,128)S(1)} fusion(bf16[768,512]{1,0:T(8,128)(2,1)} %bitcast.119, s32[256]{0:T(256)S(1)} %bitcast.142), kind=kOutput, calls=%fused_computation.4 | convolution fusion | flops 201523200 | bytes 1311744 | tf_op jit(solution)/shard_map/dot_general | solution.py:490
  151.8 0.1 fusion.1
  151.9 0.8 add_convert_fusion
  (39 shorter events, 0.5 us)
Async XLA Ops:
  0.0 43.5 %copy-start = (bf16[256,2048]{1,0:T(8,128)(2,1)S(1)}, bf16[256,2048]{1,0:T(8,128)(2,1)}, u32[]{:S(2)}) copy-start(bf16[256,2048]{1,0:T(8,128)(2,1)} %param.16) | copy-start | bytes 3145732
  3.7 1.0 copy-start.4
  4.9 1.5 copy-start.2
  32.8 4.6 %copy-start.1 = (f32[256,4,128]{2,1,0:T(4,128)S(1)}, f32[256,4,128]{2,1,0:T(4,128)}, u32[]{:S(2)}) copy-start(f32[256,4,128]{2,1,0:T(4,128)} %get-tuple-element.19) | copy-start | bytes 1572868
  38.4 1.0 copy-start.3
  38.4 1.1 copy-start.10
  38.4 2.1 %copy-start.7 = (s32[256,2]{0,1:T(2,128)S(1)}, s32[256,2]{0,1:T(2,128)}, u32[]{:S(2)}) copy-start(s32[256,2]{0,1:T(2,128)} %param.29) | copy-start | bytes 6148
  45.6 103.0 %copy-start.6 = (s32[256,2]{0,1:T(2,128)S(1)}, s32[256,2]{0,1:T(2,128)}, u32[]{:S(2)}) copy-start(s32[256,2]{0,1:T(2,128)} %fusion.58) | copy-start | bytes 6148
  148.5 3.2 %copy-start.8 = (f32[256,2]{0,1:T(2,128)S(1)}, f32[256,2]{0,1:T(2,128)}, u32[]{:S(2)}) copy-start(f32[256,2]{0,1:T(2,128)} %param.31) | copy-start | bytes 6148
  148.5 3.2 %copy-start.9 = (f32[256]{0:T(256)S(1)}, f32[256]{0:T(256)}, u32[]{:S(2)}) copy-start(f32[256]{0:T(256)} %param.30) | copy-start | bytes 3076
  148.6 3.4 %copy-start.5 = (bf16[256,512]{1,0:T(8,128)(2,1)S(1)}, bf16[256,512]{1,0:T(8,128)(2,1)}, u32[]{:S(2)}) copy-start(bf16[256,512]{1,0:T(8,128)(2,1)} %get-tuple-element.7) | copy-start | bytes 786436

commit v2 on v1

--- a/solution.py
+++ b/solution.py
@@ -158,11 +158,12 @@
     ]
     barrier = pltpu.get_barrier_semaphore()
 
+    square = tp_size == 4 and group % 2 == 0
+
     def tp_of(j):
-        return lax.rem(my_t + j, tp_size)
-
-    def tp_from(j):
-        return lax.rem(my_t + tp_size - j, tp_size)
+        if not square:
+            return lax.rem(my_t + j, tp_size)
+        return (my_t, my_t + 1 - 2 * lax.rem(my_t, 2), lax.rem(my_t + 2, 4), 3 - my_t)[j]
 
     def sp_of(k):
         return lax.rem(my_s + k, sp_size)
@@ -255,12 +256,28 @@
         )
 
 
+    ag_peers = 3 if square else tp_size
+    half = group // 2
+
+    def relays(g):
+        first = arr.at[tp_of(1), pl.ds(g * group, half)]
+        second = arr.at[tp_of(2), pl.ds(g * group + half, half)]
+        return (
+            push(first, first, ag_send.at[3, g], ag_recv.at[3, g], {"tp": tp_of(2)}),
+            push(second, second, ag_send.at[0, g], ag_recv.at[0, g], {"tp": tp_of(1)}),
+        )
+
+    def relay(g):
+        for j, copy in zip((1, 2), relays(g)):
+            ag_copy(g, j).wait_recv()
+            copy.start()
+
     def dispatch(g):
         def take(i):
             out_copy(g * group + i).wait_recv()
 
         each(1 if isinstance(g, int) and g == 0 else 0, group, take)
-        each(1, tp_size, lambda j: ag_copy(g, j).start())
+        each(1, ag_peers, lambda j: ag_copy(g, j).start())
 
     dispatch(0)
     each(1, groups, dispatch)
@@ -268,9 +285,23 @@
         load.wait()
     tile = min(256, hidden_width)
 
+    ahead = min(2, groups)
+    if square:
+        for g in range(ahead):
+            relay(g)
+
     @pl.loop(0, groups)
     def _(g):
-        each(1, tp_size, lambda j: ag_copy(g, j).wait_recv())
+        if square:
+
+            @pl.when(g + ahead < groups)
+            def _():
+                relay(g + ahead)
+
+            for copy in relays(g):
+                copy.wait_recv()
+        else:
+            each(1, tp_size, lambda j: ag_copy(g, j).wait_recv())
 
         @pl.loop(0, hidden_width // tile)
         def _(f):
@@ -314,10 +345,14 @@
     def drain(j):
         pj_copy(j).wait_send()
         for g in range(groups):
-            ag_copy(g, j).wait_send()
             rs_copy(g, j).wait_send()
 
     each(1, tp_size, drain)
+    for g in range(groups):
+        each(1, ag_peers, lambda j: ag_copy(g, j).wait_send())
+        if square:
+            for copy in relays(g):
+                copy.wait_send()
 
 
 def run_experts(mixer_out, projection, skip_cols, gain_cols, places, gate, up, down, cap):

time: 153 us -> 154 us (level)
  no operation moved by 1% of the time
where the time goes in v2:
time: 154 us; the launch traced here: 153 us
  Pallas kernels  122 us (79%)
  local copies, waits for them, and re-layouts  13 us (8%)
  other arithmetic  10.4 us (7%)
  matrix products  7.53 us (5%)
    pallas_call x1, Pallas kernels, run_experts(): pl.pallas_call(functools.partial(expert_kernel, sp_size, tp_size, group),...  104 us
    pallas_call x1, Pallas kernels, gather_states(): pl.pallas_call(functools.partial(state_kernel, sp_size), out_shape=jax.Sh...  18.5 us
    convert_element_type x7, local copies, waits for them, and re-layouts, carry_states(): held = states[lap].astype(jnp.float32) * factor[:, :, None]  4.54 us
    dot_general x2, matrix products, shards(): jnp.dot((places[:, j:j + 1] == slot_ids).astype(jnp.bfloat16), returned,...  3.13 us

profile of v2, /device:TPU:0, one launch (start us, length us, event | category | flops | bytes accessed | tf_op | source)
XLA Modules:
  0.0 153.5 jit_solution(3501384514022599062)
XLA Ops:
  0.0 1.2 copy.54
  1.2 0.7 broadcast_subtract_fusion.1
  1.9 0.9 broadcast_subtract_fusion
  2.8 0.7 add_bitcast_fusion
  3.5 0.2 copy.55
  3.7 0.4 fusion.7
  4.2 0.1 copy.57
  4.4 0.2 copy.79
  4.7 0.1 copy.52
  4.8 0.1 convert_multiply_fusion
  5.0 0.2 copy.78
  5.2 1.2 broadcast_multiply_fusion
  6.4 0.7 convolution_convert_fusion
  7.1 0.8 maximum_maximum_fusion.own_ref
  7.9 18.5 %shard_map.154 = bf16[8,528,128]{2,1,0:T(8,128)(2,1)} custom-call(bf16[528,128]{1,0:T(8,128)(2,1)} %maximum_maximum_fusion.own_ref), custom_call_target="tpu_custom_call" | custom-call | tf_op jit(solution)/shard_map/pallas_call | solution.py:95
  26.4 0.7 slice_convert_fusion
  27.2 0.6 multiply_select_fusion
  27.7 0.9 convert_select_fusion
  28.7 0.1 copy.65
  28.8 2.0 %fusion.66 = (bf16[1,512,128]{2,1,0:T(8,128)(2,1)S(1)}, bf16[1,512,128]{2,1,0:T(8,128)(2,1)S(1)}, bf16[1,512,128]{2,1,0:T(8,128)(2,1)}, bf16[1,512,128]{2,1,0:T(...) fusion(bf16[8,528,128]{2,1,0:T(8,128)(2,1)} %shard_map.154), kind=kLoop, calls=%fused_computation.118 | loop fusion | bytes 1835008 | tf_op jit(solution)/shard_map/slice | solution.py:429
  30.8 0.1 copy.64
  30.9 0.1 copy.66
  31.0 0.1 copy.67
  31.1 0.8 copy.68
  31.9 0.8 copy.69
  32.8 1.8 %copy.70 = f32[4,128,128]{1,2,0:T(8,128)} copy(bf16[4,128,128]{2,1,0:T(8,128)(2,1)} %bitcast.131) | data formatting | bytes 393216 | tf_op jit(solution)/shard_map/convert_element_type | solution.py:429
  34.5 0.8 copy.71
  35.3 2.0 %convolution_bitcast_fusion = f32[256,4,128]{0,2,1:T(8,128)S(1)} fusion(f32[256,4,128]{2,1,0:T(4,128)S(1)} %get-tuple-element.27, f32[4,128,128]{1,2,0:T(8,128)} %copy.71, f32[4,128,128]{1,2,0:T(8,128)} %copy.70, f32[4,128,128]{1,2,0:T(8,128)} %copy.69, f32[4,128,128]{1,2,0:T(8,128)} %copy.68, f32[4,128,128]{1,2,0:T(8,128)S(1)} %copy.67, ...), kind=kOutput, calls=%fused_computation.1 | convolution fusion | flops 202702848 | bytes 3160071 | tf_op jit(solution)/shard_map/thd,hdv->thv/dot_general | solution.py:479
  37.4 1.0 convolution_select_fusion
  38.4 0.7 multiply_reduce_fusion
  39.2 0.2 copy-done.3
  39.4 0.1 copy.73
  39.5 0.2 multiply_convert_fusion
  39.7 0.8 copy.80.mixer_ref
  40.5 0.1 copy.75
  40.7 0.1 eq.59
  40.8 1.3 reduce-window.16
  42.2 0.2 slice_reduce_fusion
  42.4 0.1 eq.55
  42.7 0.1 reduce_sum.31
  42.9 0.6 fusion.58
  43.5 0.7 constant_dynamic-slice_fusion.skip_ref
  44.2 1.3 dynamic_slice.7
  45.6 103.7 %shard_map.155 = (bf16[8,96,512]{2,1,0:T(8,128)(2,1)}, bf16[256,512]{1,0:T(8,128)(2,1)}) custom-call(bf16[256,512]{1,0:T(8,128)(2,1)} %copy.80.mixer_ref, bf16[512,2048]{1,0:T(8,128)(2,1)} %proj_ref.1, bf16[256,512]{1,0:T(8,128)(2,1)} %constant_dynamic-slice_fusion.skip_ref, f32[1,512]{1,0:T(1,128)} %bitcast.140, s32[2,256]{1,0:T(2,128)} %bitcast.138, ...), custom_call_target="tpu_custom_call" | custom-call | tf_op jit(solution)/shard_map/pallas_call | solution.py:368
  149.3 1.6 %convolution_bitcast_fusion.3 = f32[256,1,512]{2,0,1:T(8,128)S(1)} fusion(bf16[768,512]{1,0:T(8,128)(2,1)} %bitcast.118, s32[256]{0:T(256)S(1)} %bitcast.143), kind=kOutput, calls=%fused_computation.5 | convolution fusion | flops 201523200 | bytes 1311744 | tf_op jit(solution)/shard_map/dot_general | solution.py:525
  150.9 1.5 %convolution_bitcast_fusion.2 = f32[256,1,512]{2,0,1:T(8,128)S(1)} fusion(bf16[768,512]{1,0:T(8,128)(2,1)} %bitcast.119, s32[256]{0:T(256)S(1)} %bitcast.142), kind=kOutput, calls=%fused_computation.4 | convolution fusion | flops 201523200 | bytes 1311744 | tf_op jit(solution)/shard_map/dot_general | solution.py:525
  152.5 0.1 fusion.1
  152.7 0.8 add_convert_fusion
  (39 shorter events, 0.5 us)
Async XLA Ops:
  0.0 43.5 %copy-start = (bf16[256,2048]{1,0:T(8,128)(2,1)S(1)}, bf16[256,2048]{1,0:T(8,128)(2,1)}, u32[]{:S(2)}) copy-start(bf16[256,2048]{1,0:T(8,128)(2,1)} %param.16) | copy-start | bytes 3145732
  3.7 1.0 copy-start.4
  4.9 1.5 copy-start.2
  32.8 4.6 %copy-start.1 = (f32[256,4,128]{2,1,0:T(4,128)S(1)}, f32[256,4,128]{2,1,0:T(4,128)}, u32[]{:S(2)}) copy-start(f32[256,4,128]{2,1,0:T(4,128)} %get-tuple-element.19) | copy-start | bytes 1572868
  38.4 1.0 copy-start.3
  38.4 1.1 copy-start.10
  38.4 2.1 %copy-start.7 = (s32[256,2]{0,1:T(2,128)S(1)}, s32[256,2]{0,1:T(2,128)}, u32[]{:S(2)}) copy-start(s32[256,2]{0,1:T(2,128)} %param.29) | copy-start | bytes 6148
  45.6 103.7 %copy-start.6 = (s32[256,2]{0,1:T(2,128)S(1)}, s32[256,2]{0,1:T(2,128)}, u32[]{:S(2)}) copy-start(s32[256,2]{0,1:T(2,128)} %fusion.58) | copy-start | bytes 6148
  149.3 3.2 %copy-start.8 = (f32[256,2]{0,1:T(2,128)S(1)}, f32[256,2]{0,1:T(2,128)}, u32[]{:S(2)}) copy-start(f32[256,2]{0,1:T(2,128)} %param.31) | copy-start | bytes 6148
  149.3 3.2 %copy-start.9 = (f32[256]{0:T(256)S(1)}, f32[256]{0:T(256)}, u32[]{:S(2)}) copy-start(f32[256]{0:T(256)} %param.30) | copy-start | bytes 3076
  149.3 3.4 %copy-start.5 = (bf16[256,512]{1,0:T(8,128)(2,1)S(1)}, bf16[256,512]{1,0:T(8,128)(2,1)}, u32[]{:S(2)}) copy-start(bf16[256,512]{1,0:T(8,128)(2,1)} %get-tuple-element.7) | copy-start | bytes 786436
